TPU v7x, 32 devices: a whole 2x2x4 slice. The times are simulated.
32 devices in a mesh: ep: 8 (over z, x), tp: 4 (over y, core).
Axes of the slice: x: 2, y: 2, z: 4, core: 2. Of those that a mesh axis runs over, the one named last changes fastest.
Arguments:
- queries: bfloat16 [1024, 4096], P('ep', 'tp'), may hold values from -112 to 112
- key_rows: bfloat16 [1024, 4096], P('ep', 'tp'), may hold values from -8.1 to 8.1
- values: bfloat16 [1024, 4096], P('ep', 'tp'), may hold values from -6 to 6
- lambdas: float32 [16], P('tp'), may hold values from 0.3 to 0.8
- head_gain: float32 [256], replicated, may hold values from 0.1 to 1.9
- tokens: bfloat16 [512, 4096], P('ep'), may hold values from -6 to 6
- moe_gain: float32 [4096], replicated, may hold values from 0.1 to 1.9
- routes: int32 [512, 2], P('ep'), may hold values from 0 to 7, all different within a row; in each aligned block of 64 rows (0 to 63, 64 to 127, ...) at most 32 rows name the same one
- route_scores: float32 [512, 2], P('ep'), may hold values from -6 to 6
- w_gate: bfloat16 [8, 4096, 2048], P('ep', None, 'tp'), may hold values from -0.09375 to 0.09375
- w_up: bfloat16 [8, 4096, 2048], P('ep', None, 'tp'), may hold values from -0.09375 to 0.09375
- w_down: bfloat16 [8, 2048, 4096], P('ep', 'tp'), may hold values from -0.125 to 0.125
Outputs:
- attended: bfloat16 [1024, 4096], P('ep', 'tp')
- expert_out: bfloat16 [512, 4096], P('ep', 'tp')
Inputs may be any that keep to these rules, and one draw needn't show every extreme that they name: `routes`: each row names 2 different experts. Among the rows of one index of ep at most 32 name the same expert, and some index reaches 32 in every draw.
All inputs are finite; a program needn't handle non-finite values.
Results may differ from a plain program's by a relative error of at most 0.018.
Values may be sent and summed in bfloat16 or wider, within the bound.
A program may use at most 64 MiB of HBM per device.

v0:
```python
import jax
import jax.numpy as jnp
from jax import lax
from jax.sharding import PartitionSpec as P

QKD = 128
VD = 256
TOP = 2
neg_big = -1e30
head_eps = 1e-05
moe_eps = 1e-06
head_scale = 0.8


def slot_table(routes, experts, capacity):
    flat_routes = routes.reshape(-1)
    onehot = (flat_routes[:, None] == jnp.arange(experts, dtype=jnp.int32)[None, :]).astype(
        jnp.int32
    )
    before = jnp.cumsum(onehot, axis=0) - onehot
    position = jnp.sum(before * onehot, axis=1)
    return (flat_routes * capacity + position).reshape(routes.shape)


def fold_block(state, query_group, query_pos, key_heads, value_heads, key_pos):
    maxima, denominators, accumulated = state
    scores = jnp.einsum(
        "qhmd,khmd->hmqk", query_group, key_heads, preferred_element_type=jnp.float32
    ) * QKD ** (-0.5)
    visible = key_pos[None, :] <= query_pos[:, None]
    scores = jnp.where(visible, scores, neg_big)
    new_max = jnp.maximum(maxima, jnp.max(scores, axis=-1))
    weights = jnp.where(visible, jnp.exp(scores - new_max[..., None]), 0.0)
    accumulated = jnp.einsum(
        "hmqk,khd->hmqd", weights, value_heads, precision=lax.Precision.HIGHEST
    )
    denominators = jnp.sum(weights, axis=-1)
    return (new_max, denominators, accumulated)


def local(
    queries,
    key_rows,
    values,
    lambdas,
    head_gain,
    tokens,
    moe_gain,
    routes,
    route_scores,
    w_gate,
    w_up,
    w_down,
):
    rows_a = queries.shape[0]
    half_rows = rows_a // 2
    head_local = lambdas.shape[0]
    ep_count = lax.axis_size("ep")
    ep_index = lax.axis_index("ep")
    early_queries = queries[:half_rows]
    later_queries = queries[half_rows:]
    early_pos = ep_index * rows_a + jnp.arange(half_rows, dtype=jnp.int32)
    later_pos = ep_index * rows_a + half_rows + jnp.arange(half_rows, dtype=jnp.int32)
    query_groups = (
        early_queries.reshape(half_rows, head_local, 2, QKD),
        later_queries.reshape(half_rows, head_local, 2, QKD),
    )
    position_groups = (early_pos, later_pos)
    start_state = (
        jnp.full((head_local, 2, half_rows), neg_big, jnp.float32),
        jnp.zeros((head_local, 2, half_rows), jnp.float32),
        jnp.zeros((head_local, 2, half_rows, VD), jnp.float32),
    )
    totals = (start_state, start_state)
    row_start = jnp.int32(0)
    key_block = lax.all_gather(key_rows, "ep", axis=0, tiled=True)
    value_block = lax.all_gather(values, "ep", axis=0, tiled=True)
    key_count = key_block.shape[0]
    key_heads = key_block.reshape(key_count, head_local, 2, QKD)
    value_heads = value_block.reshape(key_count, head_local, VD).astype(jnp.float32)
    key_pos = jnp.arange(key_count, dtype=jnp.int32)
    updated = []
    for attend_group_index in range(2):
        state = totals[attend_group_index]
        query_group = query_groups[attend_group_index]
        query_pos = position_groups[attend_group_index]
        state = lax.cond(
            row_start <= query_pos[-1],
            lambda held: fold_block(held, query_group, query_pos, key_heads, value_heads, key_pos),
            lambda held: held,
            state,
        )
        updated.append(state)
    folded = (updated[0], updated[1])
    attended_groups = []
    for group_index in range(2):
        maxima, denominators, accumulated = folded[group_index]
        mixed_out = (
            accumulated[:, 0] / denominators[:, 0, :, None]
            - lambdas[:, None, None] * accumulated[:, 1] / denominators[:, 1, :, None]
        )
        scaled = mixed_out * lax.rsqrt(
            jnp.mean(mixed_out * mixed_out, axis=-1, keepdims=True) + head_eps
        )
        scaled = scaled * head_gain * head_scale
        attended_groups.append(
            scaled.transpose(1, 0, 2).reshape(half_rows, head_local * VD).astype(jnp.bfloat16)
        )
    later_out = attended_groups[1]
    attended = jnp.concatenate([attended_groups[0], later_out], axis=0)
    rows_b = tokens.shape[0]
    capacity = 2 * TOP * rows_b // ep_count
    token_f32 = tokens.astype(jnp.float32)
    normed = (
        token_f32
        * lax.rsqrt(jnp.mean(token_f32 * token_f32, axis=-1, keepdims=True) + moe_eps)
        * moe_gain
    ).astype(jnp.bfloat16)
    gate_weights = jax.nn.softmax(route_scores, axis=-1)
    slot_of = slot_table(routes, ep_count, capacity)
    row_ids = jnp.broadcast_to(jnp.arange(rows_b, dtype=jnp.int32)[:, None], slot_of.shape)
    row_of_slot = (
        jnp.zeros((ep_count * capacity,), jnp.int32)
        .at[slot_of.reshape(-1)]
        .set(row_ids.reshape(-1))
    )
    gate_local = w_gate[0]
    up_local = w_up[0]
    down_local = w_down[0]
    outgoing = normed[row_of_slot]
    arrived = lax.all_to_all(outgoing, "ep", split_axis=0, concat_axis=0, tiled=True)
    gate_act = jnp.dot(arrived, gate_local, preferred_element_type=jnp.float32)
    up_act = jnp.dot(arrived, up_local, preferred_element_type=jnp.float32)
    hidden = (jax.nn.silu(gate_act) * up_act).astype(jnp.bfloat16)
    summed = lax.psum_scatter(
        lax.dot_general(
            down_local, hidden, (((0,), (1,)), ((), ())), preferred_element_type=jnp.float32
        ).astype(jnp.bfloat16),
        "tp",
        scatter_dimension=0,
        tiled=True,
    )
    returned = lax.all_to_all(summed, "ep", split_axis=1, concat_axis=1, tiled=True)
    slot_ids = jnp.arange(ep_count * capacity, dtype=jnp.int32)
    combined = jnp.zeros((rows_b, returned.shape[0]), jnp.float32)
    for choice_index in range(TOP):
        picker = (slot_of[:, choice_index, None] == slot_ids[None, :]).astype(jnp.bfloat16)
        picked = lax.dot_general(
            picker, returned, (((1,), (1,)), ((), ())), preferred_element_type=jnp.float32
        )
        combined = combined + gate_weights[:, choice_index, None] * picked
    expert_out = combined.astype(jnp.bfloat16)
    return (attended, expert_out)


def solution(mesh):
    return jax.shard_map(
        local,
        mesh=mesh,
        in_specs=(
            P("ep", "tp"),
            P("ep", "tp"),
            P("ep", "tp"),
            P("tp"),
            P(),
            P("ep", None),
            P(),
            P("ep", None),
            P("ep", None),
            P("ep", None, "tp"),
            P("ep", None, "tp"),
            P("ep", "tp", None),
        ),
        out_specs=(P("ep", "tp"), P("ep", "tp")),
        check_vma=False,
    )
```

profile of v0, /device:TPU:0, one launch (start us, length us, event | category | flops | bytes accessed | tf_op | source)
XLA Modules:
  0.0 190.7 jit_solution(13893074613434656306)
XLA Ops:
  8.1 1.9 copy.24
  9.9 0.8 copy.34
  11.8 1.0 scatter_custom_fusion
  12.8 1.2 fusion.42
  14.0 0.9 fusion.44
  15.0 3.2 %gather_fusion = bf16[256,4096]{1,0:T(8,128)(2,1)} fusion(bf16[64,4096]{1,0:T(8,128)(2,1)S(1)} %fusion.44, s32[1024]{0:T(1024)S(1)} %pad_clamp_fusion), kind=kCustom, calls=%fused_computation | custom fusion | bytes 4195328 | tf_op jit(solution)/shard_map/gather | solution.py:130
  18.2 7.4 %all-to-all-start = ((bf16[8,32,4096]{2,1,0:T(8,128)(2,1)}), bf16[8,32,4096]{2,1,0:T(8,128)(2,1)S(1)}, u32[]{:S(2)}, u32[]{:S(2)}) async-start(bf16[8,32,4096]{2,1,0:T(8,128)(2,1)} %bitcast.20), calls=%async_computation | async-start | bytes 4194304 | tf_op jit(solution)/shard_map/all_to_all | solution.py:131
  25.6 0.8 copy.23
  26.5 69.8 %all-to-all-done = bf16[8,32,4096]{2,1,0:T(8,128)(2,1)S(1)} async-done(((bf16[8,32,4096]{2,1,0:T(8,128)(2,1)}), bf16[8,32,4096]{2,1,0:T(8,128)(2,1)S(1)}, u32[]{:S(2)}, u32[]{:S(2)}) %all-to-all-start) | async-done | bytes 2097184 | tf_op jit(solution)/shard_map/all_to_all | solution.py:131
  96.3 3.5 %fusion.32 = f32[256,512]{1,0:T(8,128)S(1)} fusion(bf16[256,4096]{1,0:T(8,128)(2,1)S(1)} %bitcast.99, bf16[1,4096,512]{2,1,0:T(8,128)(2,1)} %param.25), kind=kOutput, calls=%fused_computation.43 | convolution fusion | flops 1073741824 | bytes 6815744 | tf_op jit(solution)/shard_map/dot_general | solution.py:132
  99.8 7.4 %fusion.28 = bf16[4096,256]{0,1:T(8,128)(2,1)} fusion(bf16[1,512,4096]{2,1,0:T(8,128)(2,1)} %param.27, bf16[256,4096]{1,0:T(8,128)(2,1)S(1)} %bitcast.100, bf16[1,4096,512]{2,1,0:T(8,128)(2,1)} %param.26, f32[256,512]{1,0:T(8,128)S(1)} %fusion.32), kind=kOutput, calls=%fused_computation.39 | convolution fusion | flops 2149318656 | bytes 13107200 | tf_op jit(solution)/shard_map/dot_general | solution.py:136
  110.0 4.1 %convert.3 = f32[1024,4,256]{0,2,1:T(8,128)} convert(bf16[1024,4,256]{0,2,1:T(8,128)(2,1)} %bitcast.98) | non-fusion elementwise | flops 1048576 | bytes 6291456 | tf_op jit(solution)/shard_map/convert_element_type | solution.py:80
  114.1 33.2 %all-gather.3.cloned.1.call-done = bf16[1024,1024]{0,1:T(8,128)(2,1)} async-done(((bf16[128,1024]{0,1:T(8,128)(2,1)}), bf16[1024,1024]{0,1:T(8,128)(2,1)}) %all-gather.3.cloned.1.call-update) | async-done | bytes 2097168 | tf_op jit(solution)/shard_map/all_gather | solution.py:76
  147.3 8.6 %conditional.3 = (f32[4,2,64]{2,1,0:T(2,128)S(1)}, f32[4,2,64,256]{3,2,1,0:T(8,128)S(1)}) conditional(s32[]{:T(128)} %bitcast.10, () %tuple.26, (s32[1024]{0:T(1024)S(1)}, s32[64]{0:T(128)S(1)}, bf16[128,1024]{1,0:T(8,128)(2,1)S(1)}, bf16[1024,4,2,128]{0,3,2,1:T(8,128)(2,1)}, f32[1024,4,256]{0,2,1:T(8,128)}) %tuple.56), branch_computations={%region_5.6_spmd, %region_6.9_spmd} | conditional | flops 1751186944 | bytes 30818604 | solution.py:87
  147.5 2.4 %fusion.16 = (f32[4,2,64]{2,1,0:T(2,128)S(1)}, f32[4,2,64,1024]{3,2,1,0:T(8,128)S(1)}) fusion(pred[64,1024]{1,0:T(8,128)(4,1)S(1)} %broadcast_compare_fusion.1, bf16[1024,4,2,128]{0,3,2,1:T(8,128)(2,1)} %get-tuple-element.52, bf16[64,4,2,128]{3,2,1,0:T(2,128)(2,1)S(1)} %reshape.109), kind=kOutput, calls=%fused_computation.24 | convolution fusion | flops 135790080 | bytes 4392960 | tf_op jit(solution)/shard_map/cond/branch_1_fun/qhmd,khmd->hmqk/dot_general | solution.py:27
  150.3 4.8 %fusion.14 = f32[4,2,64,256]{3,2,1,0:T(8,128)S(1)} fusion(f32[1024,4,256]{0,2,1:T(8,128)S(1)} %copy-done, f32[4,2,64,1024]{3,2,1,0:T(8,128)S(1)} %get-tuple-element.63, f32[4,2,64]{2,1,0:T(2,128)S(1)} %broadcast_maximum_fusion.1, pred[64,1024]{1,0:T(8,128)(4,1)S(1)} %broadcast_compare_fusion.1), kind=kOutput, calls=%fused_computation.20 | convolution fusion | flops 1612709888 | bytes 6883328 | tf_op jit(solution)/shard_map/cond/branch_1_fun/hmqk,khd->hmqd/dot_general | solution.py:34
  155.2 0.7 fusion.17
  155.9 8.8 %conditional.2 = (f32[4,2,64]{2,1,0:T(2,128)S(1)}, f32[4,2,64,256]{3,2,1,0:T(8,128)S(1)}) conditional(s32[]{:T(128)} %bitcast.2, () %tuple.24, (s32[1024]{0:T(1024)S(1)}, s32[64]{0:T(128)S(1)}, bf16[128,1024]{1,0:T(8,128)(2,1)S(1)}, bf16[1024,4,2,128]{0,3,2,1:T(8,128)(2,1)}, f32[1024,4,256]{0,2,1:T(8,128)}) %tuple.57), branch_computations={%region_0.0_spmd, %region_1.4_spmd} | conditional | flops 1751186944 | bytes 30818604 | solution.py:87
  156.3 2.4 %fusion.2 = (f32[4,2,64]{2,1,0:T(2,128)S(1)}, f32[4,2,64,1024]{3,2,1,0:T(8,128)S(1)}) fusion(pred[64,1024]{1,0:T(8,128)(4,1)S(1)} %broadcast_compare_fusion, bf16[1024,4,2,128]{0,3,2,1:T(8,128)(2,1)} %get-tuple-element.47, bf16[64,4,2,128]{3,2,1,0:T(2,128)(2,1)S(1)} %reshape.108), kind=kOutput, calls=%fused_computation.6 | convolution fusion | flops 135790080 | bytes 4392960 | tf_op jit(solution)/shard_map/cond/branch_1_fun/qhmd,khmd->hmqk/dot_general | solution.py:27
  159.1 4.8 %fusion = f32[4,2,64,256]{3,2,1,0:T(8,128)S(1)} fusion(f32[1024,4,256]{0,2,1:T(8,128)S(1)} %copy-done.1, f32[4,2,64,1024]{3,2,1,0:T(8,128)S(1)} %get-tuple-element.61, f32[4,2,64]{2,1,0:T(2,128)S(1)} %broadcast_maximum_fusion, pred[64,1024]{1,0:T(8,128)(4,1)S(1)} %broadcast_compare_fusion), kind=kOutput, calls=%fused_computation.2 | convolution fusion | flops 1612709888 | bytes 6883328 | tf_op jit(solution)/shard_map/cond/branch_1_fun/hmqk,khd->hmqd/dot_general | solution.py:34
  164.7 3.5 %all-to-all-start.1 = ((bf16[1024,8,32]{0,2,1:T(8,128)(2,1)}), bf16[1024,8,32]{0,2,1:T(8,128)(2,1)S(1)}, u32[]{:S(2)}, u32[]{:S(2)}) async-start(bf16[1024,8,32]{0,2,1:T(8,128)(2,1)} %bitcast.101), calls=%async_computation.2 | async-start | bytes 1048576 | tf_op jit(solution)/shard_map/all_to_all | solution.py:143
  168.8 0.7 pad_maximum_fusion
  169.5 12.6 %all-to-all-done.1 = bf16[1024,8,32]{0,2,1:T(8,128)(2,1)S(1)} async-done(((bf16[1024,8,32]{0,2,1:T(8,128)(2,1)}), bf16[1024,8,32]{0,2,1:T(8,128)(2,1)S(1)}, u32[]{:S(2)}, u32[]{:S(2)}) %all-to-all-start.1) | async-done | bytes 524320 | tf_op jit(solution)/shard_map/all_to_all | solution.py:143
  182.4 0.9 fusion.41
  (65 shorter events, 5.3 us)
Async XLA Ops:
  8.0 6.0 %copy-start.2 = (bf16[64,4096]{1,0:T(8,128)(2,1)S(1)}, bf16[64,4096]{1,0:T(8,128)(2,1)}, u32[]{:S(2)}) copy-start(bf16[64,4096]{1,0:T(8,128)(2,1)} %param.21) | copy-start | bytes 1572868
  8.0 102.0 %all-gather.5.cloned.1.call-start = ((), (), s32[]{:S(2)}) async-start(), calls=%async_computation.4 | async-start | bytes 2359296 | tf_op jit(solution)/shard_map/all_gather | solution.py:77
  18.2 7.5 %copy-start.3 = (bf16[128,1024]{1,0:T(8,128)(2,1)S(1)}, bf16[128,1024]{1,0:T(8,128)(2,1)}, u32[]{:S(2)}) copy-start(bf16[128,1024]{1,0:T(8,128)(2,1)} %param.17) | copy-start | bytes 786436
  18.2 78.2 %all-to-all-start = ((bf16[8,32,4096]{2,1,0:T(8,128)(2,1)}), bf16[8,32,4096]{2,1,0:T(8,128)(2,1)S(1)}, u32[]{:S(2)}, u32[]{:S(2)}) async-start(bf16[8,32,4096]{2,1,0:T(8,128)(2,1)} %bitcast.20), calls=%async_computation | async-start | bytes 4194304 | tf_op jit(solution)/shard_map/all_to_all | solution.py:131
  25.6 121.7 %all-gather.3.cloned.1.call-start = ((), (), s32[]{:S(2)}) async-start(), calls=%async_computation.3 | async-start | bytes 2359296 | tf_op jit(solution)/shard_map/all_gather | solution.py:76
  26.5 138.2 %reduce-scatter.2.cloned.1.call-start = ((), (), s32[]{:S(2)}) async-start(), calls=%async_computation.5 | async-start | bytes 2621440 | tf_op jit(solution)/shard_map/reduce_scatter | solution.py:135
  107.2 2.5 %copy-start.5 = (f32[64,2]{0,1:T(2,128)S(1)}, f32[64,2]{0,1:T(2,128)}, u32[]{:S(2)}) copy-start(f32[64,2]{0,1:T(2,128)} %param.24) | copy-start | bytes 1540
  110.0 37.3 %copy-start.4 = (bf16[128,1024]{1,0:T(8,128)(2,1)S(1)}, bf16[128,1024]{1,0:T(8,128)(2,1)}, u32[]{:S(2)}) copy-start(bf16[128,1024]{1,0:T(8,128)(2,1)} %param.16) | copy-start | bytes 786436
  147.5 2.8 %copy-start = (f32[1024,4,256]{0,2,1:T(8,128)S(1)}, f32[1024,4,256]{0,2,1:T(8,128)}, u32[]{:S(2)}) copy-start(f32[1024,4,256]{0,2,1:T(8,128)} %get-tuple-element.53) | copy-start | bytes 12582916 | tf_op jit(solution)/shard_map/cond
  155.9 12.4 %copy-start.7 = (f32[4]{0:T(128)S(1)}, f32[4]{0:T(128)}, u32[]{:S(2)}) copy-start(f32[4]{0:T(128)} %param.19) | copy-start | bytes 52
  156.3 2.8 %copy-start.1 = (f32[1024,4,256]{0,2,1:T(8,128)S(1)}, f32[1024,4,256]{0,2,1:T(8,128)}, u32[]{:S(2)}) copy-start(f32[1024,4,256]{0,2,1:T(8,128)} %get-tuple-element.48) | copy-start | bytes 12582916 | tf_op jit(solution)/shard_map/cond
  164.7 4.0 %copy-start.6 = (f32[256]{0:T(256)S(1)}, f32[256]{0:T(256)}, u32[]{:S(2)}) copy-start(f32[256]{0:T(256)} %param.20) | copy-start | bytes 3076
  164.7 17.4 %all-to-all-start.1 = ((bf16[1024,8,32]{0,2,1:T(8,128)(2,1)}), bf16[1024,8,32]{0,2,1:T(8,128)(2,1)S(1)}, u32[]{:S(2)}, u32[]{:S(2)}) async-start(bf16[1024,8,32]{0,2,1:T(8,128)(2,1)} %bitcast.101), calls=%async_computation.2 | async-start | bytes 1048576 | tf_op jit(solution)/shard_map/all_to_all | solution.py:143
Sparse Core Ops, SparseCore 0:
  10.9 83.9 all-gather.4
  97.5 49.7 all-gather.2
Sparse Core Ops, SparseCore 1:
  107.3 30.1 reduce-scatter.1
where the time goes:
time: 191 us
  waiting for transfers between devices  116 us (61%)
  matrix products  26.5 us (14%)
  between operations  17.1 us (9%)
  starting transfers between devices  11 us (6%)
  local copies, waits for them, and re-layouts  10.5 us (5%)
  other arithmetic  9.63 us (5%)
    all_to_all x1, waiting for transfers between devices, local(): lax.all_to_all(outgoing, 'ep', split_axis=0, concat_axis=0, tiled=True)  69.8 us
    all_gather x1, waiting for transfers between devices, local(): key_block = lax.all_gather(key_rows, 'ep', axis=0, tiled=True)  33.2 us
    all_to_all x1, waiting for transfers between devices, local(): lax.all_to_all(summed, 'ep', split_axis=1, concat_axis=1, tiled=True)  12.6 us
    dot_general x2, matrix products, fold_block(): jnp.einsum('hmqk,khd->hmqd', weights, value_heads, precision=lax.Precisio...  9.67 us
    all_to_all x1, starting transfers between devices, local(): lax.all_to_all(outgoing, 'ep', split_axis=0, concat_axis=0, tiled=True)  7.41 us
    dot_general x1, matrix products, local(): lax.dot_general(down_local, hidden, (((0,), (1,)), ((), ())), preferred_e...  7.37 us
    dot_general x2, matrix products, fold_block(): jnp.einsum('qhmd,khmd->hmqk', query_group, key_heads, preferred_element_t...  4.85 us
    convert_element_type x1, other arithmetic, local(): value_block.reshape(key_count, head_local, VD).astype(jnp.float32)  4.08 us
  transfers between devices with their start and end apart: 5, of which 3 were waited for; matrix products, arithmetic and copies ran while one was open for 22% of the time, Pallas kernels for 0%

commit v1 on v0

--- a/solution.py
+++ b/solution.py
@@ -73,8 +73,9 @@
     )
     totals = (start_state, start_state)
     row_start = jnp.int32(0)
-    key_block = lax.all_gather(key_rows, "ep", axis=0, tiled=True)
-    value_block = lax.all_gather(values, "ep", axis=0, tiled=True)
+    outer = jnp.concatenate([key_rows, values], axis=1)
+    tall = lax.all_gather(outer, axis_name="ep", axis=0, tiled=True)
+    key_block, value_block = jnp.split(tall, [key_rows.shape[1]], axis=1)
     key_count = key_block.shape[0]
     key_heads = key_block.reshape(key_count, head_local, 2, QKD)
     value_heads = value_block.reshape(key_count, head_local, VD).astype(jnp.float32)

time: 191 us -> 185 us (0.969)
  blocking collectives: 0 us -> 99.9 us
  waiting for transfers between devices: 116 us -> 18.7 us
  starting transfers between devices: 11 us -> 5.59 us
  matrix products: 26.5 us -> 21.3 us
  local copies, waits for them, and re-layouts: 10.5 us -> 14.6 us
  other arithmetic: 9.63 us -> 7.05 us
    all_to_all x0 -> x1, blocking collectives: none -> 99.9 us  [local(): lax.all_to_all(outgoing, 'ep', split_axis=0, concat_axis=0, tiled=True)]
    all_to_all x1 -> x0, waiting for transfers between devices: 69.8 us -> none  [local(): lax.all_to_all(outgoing, 'ep', split_axis=0, concat_axis=0, tiled=True)]
    all_gather x2 -> x1, waiting for transfers between devices: 33.2 us -> 0.02 us  [local(): tall = lax.all_gather(outer, axis_name='ep', axis=0, tiled=True)]
    all_to_all x1 -> x0, starting transfers between devices: 7.41 us -> none  [local(): lax.all_to_all(outgoing, 'ep', split_axis=0, concat_axis=0, tiled=True)]
    reduce_scatter x1, waiting for transfers between devices: 0.03 us -> 5.68 us  [local(): lax.psum_scatter(lax.dot_general(down_local, hidden, (((0,), (1,)), ((),...]
    dot_general x2, matrix products: 4.85 us -> 1.39 us  [fold_block(): jnp.einsum('qhmd,khmd->hmqk', query_group, key_heads, preferred_element_t...]
    split x0 -> x1, local copies, waits for them, and re-layouts: none -> 3.01 us  [local(): key_block, value_block = jnp.split(tall, [key_rows.shape[1]], axis=1)]
    dot_general x1, matrix products: 3.5 us -> 1.24 us  [local(): gate_act = jnp.dot(arrived, gate_local, preferred_element_type=jnp.float32)]
  transfers between devices with their start and end apart: 5 -> 3, of which waited for: 3 -> 2; matrix products, arithmetic and copies ran while one was open for 22% -> 19% of each run, Pallas kernels for 0% -> 0%
where the time goes in v1:
time: 185 us; the launch traced here: 184 us
  blocking collectives  99.9 us (54%)
  matrix products  21.3 us (12%)
  waiting for transfers between devices  18.7 us (10%)
  between operations  17.1 us (9%)
  local copies, waits for them, and re-layouts  14.6 us (8%)
  other arithmetic  7.05 us (4%)
  starting transfers between devices  5.59 us (3%)
    all_to_all x1, blocking collectives, local(): lax.all_to_all(outgoing, 'ep', split_axis=0, concat_axis=0, tiled=True)  99.9 us
    all_to_all x1, waiting for transfers between devices, local(): lax.all_to_all(summed, 'ep', split_axis=1, concat_axis=1, tiled=True)  13 us
    dot_general x2, matrix products, fold_block(): jnp.einsum('hmqk,khd->hmqd', weights, value_heads, precision=lax.Precisio...  9.66 us
    dot_general x1, matrix products, local(): lax.dot_general(down_local, hidden, (((0,), (1,)), ((), ())), preferred_e...  7.85 us
    reduce_scatter x1, waiting for transfers between devices, local(): lax.psum_scatter(lax.dot_general(down_local, hidden, (((0,), (1,)), ((),...  5.68 us
    all_to_all x1, starting transfers between devices, local(): lax.all_to_all(summed, 'ep', split_axis=1, concat_axis=1, tiled=True)  5.51 us
    unnamed x21, local copies, waits for them, and re-layouts  3.76 us
  transfers between devices with their start and end apart: 3, of which 2 were waited for; matrix products, arithmetic and copies ran while one was open for 19% of the time, Pallas kernels for 0%

profile of v1, /device:TPU:0, one launch (start us, length us, event | category | flops | bytes accessed | tf_op | source)
XLA Modules:
  0.0 184.4 jit_solution(5833872621887674472)
XLA Ops:
  8.1 1.2 copy.23
  9.2 1.1 copy.24
  10.4 0.9 pad_maximum_fusion
  12.5 1.0 scatter_custom_fusion
  13.9 1.8 %gather_fusion = bf16[256,4096]{1,0:T(8,128)(2,1)S(1)} fusion(bf16[64,4096]{1,0:T(8,128)(2,1)S(1)} %fusion.44, s32[1024]{0:T(1024)S(1)} %pad_clamp_fusion), kind=kCustom, calls=%fused_computation | custom fusion | bytes 4195328 | tf_op jit(solution)/shard_map/gather | solution.py:131
  15.8 99.9 %all_to_all.24 = bf16[8,32,4096]{2,1,0:T(8,128)(2,1)S(1)} all-to-all(bf16[8,32,4096]{2,1,0:T(8,128)(2,1)S(1)} %bitcast.96), channel_id=1, replica_groups=mesh['ep'=8,'tp'=4] {'ep'}, dimensions={0} | all-to-all | bytes 4194304 | tf_op jit(solution)/shard_map/all_to_all | solution.py:132
  115.7 1.3 copy-done.2
  117.0 1.2 fusion.32
  118.3 7.9 %fusion.28 = bf16[4096,256]{0,1:T(8,128)(2,1)} fusion(bf16[1,512,4096]{2,1,0:T(8,128)(2,1)} %param.27, bf16[256,4096]{1,0:T(8,128)(2,1)} %bitcast.101, bf16[1,4096,512]{2,1,0:T(8,128)(2,1)} %param.26, f32[256,512]{1,0:T(8,128)S(1)} %fusion.32), kind=kOutput, calls=%fused_computation.39 | convolution fusion | flops 2149318656 | bytes 13107200 | tf_op jit(solution)/shard_map/dot_general | solution.py:137
  129.0 3.0 %fusion.74 = (bf16[1024,1024]{0,1:T(8,128)(2,1)S(1)}, bf16[1024,1024]{0,1:T(8,128)(2,1)S(1)}) fusion(bf16[1024,2048]{0,1:T(8,128)(2,1)} %all-gather.2.cloned.1.call-done), kind=kLoop, calls=%fused_computation.110 | loop fusion | bytes 8388608 | tf_op jit(solution)/shard_map/split | solution.py:78
  132.0 2.4 %convert.3 = f32[1024,4,256]{0,2,1:T(8,128)} convert(bf16[1024,4,256]{0,2,1:T(8,128)(2,1)S(1)} %bitcast.97) | non-fusion elementwise | flops 1048576 | bytes 6291456 | tf_op jit(solution)/shard_map/convert_element_type | solution.py:81
  134.4 7.9 %conditional.3 = (f32[4,2,64]{2,1,0:T(2,128)S(1)}, f32[4,2,64,256]{3,2,1,0:T(8,128)S(1)}) conditional(s32[]{:T(128)} %bitcast.10, () %tuple.26, (s32[1024]{0:T(1024)S(1)}, s32[64]{0:T(128)S(1)}, bf16[128,1024]{1,0:T(8,128)(2,1)S(1)}, bf16[1024,4,2,128]{0,3,2,1:T(8,128)(2,1)S(1)}, f32[1024,4,256]{0,2,1:T(8,128)}) %tuple.55), branch_computations={%region_5.6_spmd, %region_6.9_spmd} | conditional | flops 1751186944 | bytes 30818604 | solution.py:88
  135.3 1.5 copy-done
  136.8 4.8 %fusion.14 = f32[4,2,64,256]{3,2,1,0:T(8,128)S(1)} fusion(f32[1024,4,256]{0,2,1:T(8,128)S(1)} %copy-done, f32[4,2,64,1024]{3,2,1,0:T(8,128)S(1)} %get-tuple-element.63, f32[4,2,64]{2,1,0:T(2,128)S(1)} %broadcast_maximum_fusion.1, pred[64,1024]{1,0:T(8,128)(4,1)S(1)} %broadcast_compare_fusion.1), kind=kOutput, calls=%fused_computation.20 | convolution fusion | flops 1612709888 | bytes 6883328 | tf_op jit(solution)/shard_map/cond/branch_1_fun/hmqk,khd->hmqd/dot_general | solution.py:34
  141.6 0.7 fusion.17
  142.3 8.0 %conditional.2 = (f32[4,2,64]{2,1,0:T(2,128)S(1)}, f32[4,2,64,256]{3,2,1,0:T(8,128)S(1)}) conditional(s32[]{:T(128)} %bitcast.2, () %tuple.24, (s32[1024]{0:T(1024)S(1)}, s32[64]{0:T(128)S(1)}, bf16[128,1024]{1,0:T(8,128)(2,1)S(1)}, bf16[1024,4,2,128]{0,3,2,1:T(8,128)(2,1)S(1)}, f32[1024,4,256]{0,2,1:T(8,128)}) %tuple.56), branch_computations={%region_0.0_spmd, %region_1.4_spmd} | conditional | flops 1751186944 | bytes 30818604 | solution.py:88
  143.3 1.5 copy-done.1
  144.7 4.8 %fusion = f32[4,2,64,256]{3,2,1,0:T(8,128)S(1)} fusion(f32[1024,4,256]{0,2,1:T(8,128)S(1)} %copy-done.1, f32[4,2,64,1024]{3,2,1,0:T(8,128)S(1)} %get-tuple-element.61, f32[4,2,64]{2,1,0:T(2,128)S(1)} %broadcast_maximum_fusion, pred[64,1024]{1,0:T(8,128)(4,1)S(1)} %broadcast_compare_fusion), kind=kOutput, calls=%fused_computation.2 | convolution fusion | flops 1612709888 | bytes 6883328 | tf_op jit(solution)/shard_map/cond/branch_1_fun/hmqk,khd->hmqd/dot_general | solution.py:34
  149.6 0.7 fusion.3
  150.3 5.7 %reduce-scatter.2.cloned.1.call-done = bf16[1024,256]{0,1:T(8,128)(2,1)} async-done(((bf16[4096,256]{0,1:T(8,128)(2,1)}), bf16[1024,256]{0,1:T(8,128)(2,1)}) %reduce-scatter.2.cloned.1.call-update) | async-done | bytes 524304 | tf_op jit(solution)/shard_map/reduce_scatter | solution.py:136
  156.0 5.5 %all-to-all-start.1 = ((bf16[1024,8,32]{0,2,1:T(8,128)(2,1)}), bf16[1024,8,32]{0,2,1:T(8,128)(2,1)S(1)}, u32[]{:S(2)}, u32[]{:S(2)}) async-start(bf16[1024,8,32]{0,2,1:T(8,128)(2,1)} %bitcast.102), calls=%async_computation.2 | async-start | bytes 1048576 | tf_op jit(solution)/shard_map/all_to_all | solution.py:144
  162.1 0.7 pad_maximum_fusion.1
  162.8 13.0 %all-to-all-done.1 = bf16[1024,8,32]{0,2,1:T(8,128)(2,1)S(1)} async-done(((bf16[1024,8,32]{0,2,1:T(8,128)(2,1)}), bf16[1024,8,32]{0,2,1:T(8,128)(2,1)S(1)}, u32[]{:S(2)}, u32[]{:S(2)}) %all-to-all-start.1) | async-done | bytes 524320 | tf_op jit(solution)/shard_map/all_to_all | solution.py:144
  176.0 0.9 fusion.41
  (69 shorter events, 5.6 us)
Async XLA Ops:
  8.0 3.3 %copy-start.8 = (s32[64,2]{0,1:T(2,128)S(1)}, s32[64,2]{0,1:T(2,128)}, u32[]{:S(2)}) copy-start(s32[64,2]{0,1:T(2,128)} %param.23) | copy-start | bytes 1540
  8.0 5.5 %copy-start.3 = (bf16[64,4096]{1,0:T(8,128)(2,1)S(1)}, bf16[64,4096]{1,0:T(8,128)(2,1)}, u32[]{:S(2)}) copy-start(bf16[64,4096]{1,0:T(8,128)(2,1)} %param.21) | copy-start | bytes 1572868
  8.0 5.7 %copy-start.5 = (f32[4096]{0:T(1024)S(1)}, f32[4096]{0:T(1024)}, u32[]{:S(2)}) copy-start(f32[4096]{0:T(1024)} %param.22) | copy-start | bytes 49156
  8.0 120.9 %all-gather.2.cloned.1.call-start = ((), (), s32[]{:S(2)}) async-start(), calls=%async_computation.3 | async-start | bytes 4718592 | tf_op jit(solution)/shard_map/all_gather | solution.py:77
  11.3 144.7 %reduce-scatter.2.cloned.1.call-start = ((), (), s32[]{:S(2)}) async-start(), calls=%async_computation.4 | async-start | bytes 2621440 | tf_op jit(solution)/shard_map/reduce_scatter | solution.py:136
  15.8 101.2 %copy-start.10 = (bf16[1,4096,512]{2,1,0:T(8,128)(2,1)S(1)}, bf16[1,4096,512]{2,1,0:T(8,128)(2,1)}, u32[]{:S(2)}) copy-start(bf16[1,4096,512]{2,1,0:T(8,128)(2,1)} %param.25) | copy-start | bytes 12582916
  115.7 1.3 copy-start.2
  126.1 2.5 %copy-start.6 = (f32[64,2]{0,1:T(2,128)S(1)}, f32[64,2]{0,1:T(2,128)}, u32[]{:S(2)}) copy-start(f32[64,2]{0,1:T(2,128)} %param.24) | copy-start | bytes 1540
  132.0 2.4 %copy-start.4 = (bf16[128,1024]{1,0:T(8,128)(2,1)S(1)}, bf16[128,1024]{1,0:T(8,128)(2,1)}, u32[]{:S(2)}) copy-start(bf16[128,1024]{1,0:T(8,128)(2,1)} %param.16) | copy-start | bytes 786436
  134.6 2.2 %copy-start = (f32[1024,4,256]{0,2,1:T(8,128)S(1)}, f32[1024,4,256]{0,2,1:T(8,128)}, u32[]{:S(2)}) copy-start(f32[1024,4,256]{0,2,1:T(8,128)} %get-tuple-element.53) | copy-start | bytes 12582916 | tf_op jit(solution)/shard_map/cond
  142.3 19.2 %copy-start.9 = (f32[4]{0:T(128)S(1)}, f32[4]{0:T(128)}, u32[]{:S(2)}) copy-start(f32[4]{0:T(128)} %param.19) | copy-start | bytes 52
  142.6 2.2 %copy-start.1 = (f32[1024,4,256]{0,2,1:T(8,128)S(1)}, f32[1024,4,256]{0,2,1:T(8,128)}, u32[]{:S(2)}) copy-start(f32[1024,4,256]{0,2,1:T(8,128)} %get-tuple-element.48) | copy-start | bytes 12582916 | tf_op jit(solution)/shard_map/cond
  150.3 11.6 %copy-start.7 = (f32[256]{0:T(256)S(1)}, f32[256]{0:T(256)}, u32[]{:S(2)}) copy-start(f32[256]{0:T(256)} %param.20) | copy-start | bytes 3076
  156.0 19.8 %all-to-all-start.1 = ((bf16[1024,8,32]{0,2,1:T(8,128)(2,1)}), bf16[1024,8,32]{0,2,1:T(8,128)(2,1)S(1)}, u32[]{:S(2)}, u32[]{:S(2)}) async-start(bf16[1024,8,32]{0,2,1:T(8,128)(2,1)} %bitcast.102), calls=%async_computation.2 | async-start | bytes 1048576 | tf_op jit(solution)/shard_map/all_to_all | solution.py:144
Sparse Core Ops, SparseCore 0:
  11.4 111.2 all-gather.1
Sparse Core Ops, SparseCore 1:
  126.2 29.7 reduce-scatter.1
